TPU v7x, 32 devices: a whole 2x2x4 slice. The times are simulated.
32 devices in a mesh: kv: 8 (over z, y), tp: 4 (over x, core).
Axes of the slice: x: 2, y: 2, z: 4, core: 2. Of those that a mesh axis runs over, the one named last changes fastest.
Arguments:
- proposals: bfloat16 [16, 4, 4096], P('kv', None, 'tp'), may hold values from -6 to 6
- input_norm_gain: float32 [4096], replicated, may hold values from 0.1 to 1.9
- query_matrix: bfloat16 [4096, 2048], P(None, 'tp'), may hold values from -0.09375 to 0.09375
- forget_gate_matrix: bfloat16 [4096, 2048], P(None, 'tp'), may hold values from -0.09375 to 0.09375
- value_matrix: bfloat16 [4096, 2048], P(None, 'tp'), may hold values from -0.09375 to 0.09375
- forget_floor_channel: float32 [2048], P('tp'), may hold values from 0.02 to 0.95
- proposal_extra_decay: float32 [16, 4, 16], P('kv', None, 'tp'), may hold values from -0.7 to 0
- prior_proposal_states: float32 [16, 4, 2048, 128], P('kv', None, 'tp'), may hold values from -4 to 4
- accepted: int32 [16], P('kv'), may hold values from 1 to 4
- output_matrix: bfloat16 [2048, 4096], P('tp', 'kv'), may hold values from -0.02734375 to 0.02734375
Outputs:
- mixer_output: bfloat16 [16, 4, 4096], P('tp', None, 'kv')
- next_states: float32 [16, 4, 2048, 128], P('kv', None, 'tp')
All inputs are finite; a program needn't handle non-finite values.
Results may differ from a plain program's by a relative error of at most 0.012.
Values may be sent and summed in bfloat16 or wider, within the bound.
A program may use at most 64 MiB of HBM per device.

v0:
```python
import jax
import jax.numpy as jnp
from jax import lax
from jax.sharding import PartitionSpec as P


def per_device(
    proposals,
    input_norm_gain,
    query_matrix,
    forget_gate_matrix,
    value_matrix,
    forget_floor_channel,
    proposal_extra_decay,
    prior_proposal_states,
    accepted,
    output_matrix,
):
    seq_count, prop_count, feature_block = proposals.shape
    row_count = seq_count * prop_count
    whole = lax.all_gather(proposals, "tp", axis=2, tiled=True)
    flat_rows = whole.reshape(row_count, whole.shape[2]).astype(jnp.float32)
    row_scale = lax.rsqrt(jnp.mean(flat_rows * flat_rows, axis=1) + 1e-06)[:, None]
    scaled = (flat_rows * input_norm_gain).astype(jnp.bfloat16)

    def project(weight):
        return (jnp.dot(scaled, weight, preferred_element_type=jnp.float32) * row_scale).astype(
            jnp.bfloat16
        )

    query_pre = project(query_matrix)
    forget_pre = project(forget_gate_matrix)
    value_pre = project(value_matrix)
    local_width = query_matrix.shape[1]
    head_dim = prior_proposal_states.shape[3]
    local_heads = local_width // head_dim
    head_shape = (seq_count, prop_count, local_heads, head_dim)
    query_act = jax.nn.silu(query_pre.astype(jnp.float32)).reshape(head_shape)
    lower_part = forget_floor_channel.reshape(local_heads, head_dim)
    forget_gate = lower_part + (1.0 - lower_part) * jax.nn.sigmoid(
        forget_pre.astype(jnp.float32).reshape(head_shape)
    )
    forget_gate_logs = jnp.log(forget_gate) + proposal_extra_decay[:, :, :, None]
    key_part = 1.0 - forget_gate
    values = value_pre.astype(jnp.float32).reshape(head_shape)
    picked = jnp.take_along_axis(
        prior_proposal_states, (accepted - 1)[:, None, None, None], axis=1
    )[:, 0]
    carried = picked.reshape(seq_count, local_heads, head_dim, head_dim)
    snapshots = []
    outputs = []
    for position in range(prop_count):
        carried = (
            jnp.exp(forget_gate_logs[:, position])[:, :, None, :] * carried
            + values[:, position][:, :, :, None] * key_part[:, position][:, :, None, :]
        )
        outputs.append(jnp.einsum("shvk,shk->shv", carried, query_act[:, position]))
        snapshots.append(carried.reshape(seq_count, local_width, head_dim))
    mixed_rows = jnp.stack(outputs, axis=1).reshape(row_count, local_width)
    gated_rows = mixed_rows.astype(jnp.bfloat16)
    weight_cols = lax.all_gather(output_matrix, "tp", axis=0, tiled=True)
    full_width = lax.all_gather(gated_rows, "tp", axis=1, tiled=True)
    every_row = jnp.dot(
        lax.all_gather(full_width, "kv", axis=0, tiled=True),
        weight_cols,
        preferred_element_type=jnp.float32,
    )
    block_rows = every_row.shape[0] // lax.axis_size("tp")
    result = lax.dynamic_slice_in_dim(every_row, lax.axis_index("tp") * block_rows, block_rows, 0)
    out_rows = result.shape[0]
    mixer_output = result.astype(jnp.bfloat16).reshape(
        out_rows // prop_count, prop_count, result.shape[1]
    )
    return (mixer_output, jnp.stack(snapshots, axis=1))


def solution(mesh):
    placed = (
        P("kv", None, "tp"),
        P(),
        P(None, "tp"),
        P(None, "tp"),
        P(None, "tp"),
        P("tp"),
        P("kv", None, "tp"),
        P("kv", None, "tp", None),
        P("kv"),
        P("tp", "kv"),
    )
    return jax.shard_map(
        per_device,
        mesh=mesh,
        in_specs=placed,
        out_specs=(P("tp", None, "kv"), P("kv", None, "tp", None)),
        check_vma=False,
    )
```

profile of v0, /device:TPU:0, one launch (start us, length us, event | category | flops | bytes accessed | tf_op | source)
XLA Modules:
  0.0 77.3 jit_solution(6053013169497285336)
XLA Ops:
  7.2 0.0 copy-start
  7.2 0.0 all-gather.2.cloned.1.call-start
  7.2 0.7 all-gather.2.cloned.1.call-update
  7.9 0.7 compare_and_fusion
  8.6 0.7 fusion.44
  9.2 6.4 %all_gather.12 = bf16[2,4,4096]{2,1,0:T(4,128)(2,1)S(1)} all-gather(bf16[2,4,1024]{2,1,0:T(4,128)(2,1)} %param.10), channel_id=1, replica_groups=mesh['kv'=8,'tp'=4] {'tp'}, dimensions={2}, use_global_device_ids=true | all-gather | bytes 81920 | tf_op jit(solution)/shard_map/all_gather | solution.py:21
  15.7 0.1 multiply_reduce_fusion
  15.9 0.1 copy.13
  15.9 0.2 or_reduce_fusion
  16.1 0.7 broadcast_subtract_fusion
  16.8 0.1 rsqrt.11
  16.9 0.7 multiply_convert_fusion
  17.7 3.1 %divide_multiply_fusion = f32[8,512]{1,0:T(8,128)S(1)} fusion(bf16[8,4096]{1,0:T(8,128)(2,1)S(1)} %multiply_convert_fusion, bf16[4096,512]{1,0:T(8,128)(2,1)} %param.12, f32[8]{0:T(128)S(1)} %rsqrt.11), kind=kOutput, calls=%fused_computation.58 | convolution fusion | flops 33583104 | bytes 4276256 | tf_op jit(solution)/shard_map/dot_general | solution.py:27
  20.8 0.0 copy-start.1
  20.8 2.9 %fusion.7 = f32[8,512]{1,0:T(8,128)S(1)} fusion(bf16[8,4096]{1,0:T(8,128)(2,1)S(1)} %multiply_convert_fusion, bf16[4096,512]{1,0:T(8,128)(2,1)} %param.14, f32[8]{0:T(128)S(1)} %rsqrt.11), kind=kOutput, calls=%fused_computation.12 | convolution fusion | flops 33566720 | bytes 4276256 | tf_op jit(solution)/shard_map/dot_general | solution.py:27
  23.8 0.5 copy-done.1
  24.3 0.0 copy-start.2
  24.3 0.0 copy-start.3
  24.3 0.7 fusion.5
  25.0 0.0 copy-done.2
  25.0 0.0 copy-done.3
  25.0 0.1 log_add_fusion
  25.1 0.0 copy-done
  25.1 0.6 gather_fusion
  25.7 0.3 fusion.45
  26.0 0.5 fusion.19
  26.5 0.6 fusion.20
  27.1 0.9 %fusion.15 = f32[2,4,1,128]{3,2,1,0:T(1,128)S(1)} fusion(f32[2,4,128,1]{2,3,1,0:T(1,128)S(1)} %bitcast.172, f32[2,4,128]{2,1,0:T(4,128)S(1)} %get-tuple-element.24, f32[2,4,128]{2,1,0:T(4,128)S(1)} %get-tuple-element.11, f32[2,4,128]{2,1,0:T(4,128)S(1)} %get-tuple-element.29, f32[2,4,128]{2,1,0:T(4,128)S(1)} %get-tuple-element.25, ...), kind=kOutput, calls=%fused_computation.28 | convolution fusion | flops 1966080 | bytes 581634 | tf_op jit(solution)/shard_map/shvk,shk->shv/dot_general | solution.py:57
  28.1 5.8 %all_gather.13 = bf16[8,2048]{1,0:T(8,128)(2,1)S(1)} all-gather(bf16[8,512]{1,0:T(8,128)(2,1)S(1)} %bitcast.164), channel_id=1, replica_groups=mesh['kv'=8,'tp'=4] {'tp'}, dimensions={1}, use_global_device_ids=true | all-gather | bytes 40960 | tf_op jit(solution)/shard_map/all_gather | solution.py:62
  33.8 31.2 %all_gather.14 = bf16[64,2048]{1,0:T(8,128)(2,1)S(1)} all-gather(bf16[8,2048]{1,0:T(8,128)(2,1)S(1)} %all_gather.13), channel_id=1, replica_groups=mesh['kv'=8,'tp'=4] {'kv'}, dimensions={0}, use_global_device_ids=true | all-gather | bytes 294912 | tf_op jit(solution)/shard_map/all_gather | solution.py:64
  65.3 0.5 fusion.11
  65.9 0.4 fusion.10
  66.3 1.5 %pad_maximum_fusion = f32[2,4,512,128]{3,2,1,0:T(8,128)} fusion(f32[2,1,512,128]{3,2,1,0:T(8,128)S(1)} %fusion.10, f32[2,1,512,128]{3,2,1,0:T(8,128)S(1)} %get-tuple-element.2, f32[2,1,512,128]{3,2,1,0:T(8,128)S(1)} %get-tuple-element.3, f32[2,1,512,128]{3,2,1,0:T(8,128)S(1)} %get-tuple-element.4), kind=kLoop, calls=%fused_computation.1 | loop fusion | flops 1572864 | bytes 4194304 | tf_op jit(solution)/shard_map/stack | solution.py:74
  67.8 0.0 all-gather.2.cloned.1.call-done
  67.8 2.1 %fusion.49 = bf16[64,512]{1,0:T(8,128)(2,1)S(1)} fusion(bf16[64,2048]{1,0:T(8,128)(2,1)S(1)} %all_gather.14, bf16[2048,512]{1,0:T(8,128)(2,1)} %all-gather.2.cloned.1.call-done), kind=kOutput, calls=%fused_computation.101 | convolution fusion | flops 134217728 | bytes 2424832 | tf_op jit(solution)/shard_map/dot_general | solution.py:63
  69.9 0.6 reshape.319
  (27 shorter events, 0.4 us)
Async XLA Ops:
  7.2 17.9 %copy-start = (f32[2,4,512,128]{3,2,1,0:T(8,128)S(1)}, f32[2,4,512,128]{3,2,1,0:T(8,128)}, u32[]{:S(2)}) copy-start(f32[2,4,512,128]{3,2,1,0:T(8,128)} %param.17) | copy-start | bytes 6291460
  7.2 60.6 %all-gather.2.cloned.1.call-start = ((), (), s32[]{:S(2)}) async-start(), calls=%async_computation | async-start | bytes 2621440 | tf_op jit(solution)/shard_map/all_gather | solution.py:61
  20.8 3.5 %copy-start.1 = (bf16[4096,512]{1,0:T(8,128)(2,1)S(1)}, bf16[4096,512]{1,0:T(8,128)(2,1)}, u32[]{:S(2)}) copy-start(bf16[4096,512]{1,0:T(8,128)(2,1)} %param.13) | copy-start | bytes 12582916
  24.3 0.7 copy-start.2
  24.3 0.7 copy-start.3
Sparse Core Ops, SparseCore 0:
  9.5 25.4 all-gather.1
where the time goes:
time: 77.7 us; the launch traced here: 77.3 us
  blocking collectives  43.4 us (56%)
  between operations  14.3 us (18%)
  matrix products  11.1 us (14%)
  other arithmetic  5.54 us (7%)
  local copies, waits for them, and re-layouts  2.28 us (3%)
    all_gather x1, blocking collectives, per_device(): lax.all_gather(full_width, 'kv', axis=0, tiled=True)  31.2 us
    dot_general x3, matrix products, project(): jnp.dot(scaled, weight, preferred_element_type=jnp.float32) * row_scale  6.72 us
    all_gather x1, blocking collectives, per_device(): whole = lax.all_gather(proposals, 'tp', axis=2, tiled=True)  6.44 us
    all_gather x1, blocking collectives, per_device(): full_width = lax.all_gather(gated_rows, 'tp', axis=1, tiled=True)  5.78 us
    dot_general x4, matrix products, per_device(): outputs.append(jnp.einsum('shvk,shk->shv', carried, query_act[:, position]))  2.3 us
    dot_general x1, matrix products, per_device(): jnp.dot(lax.all_gather(full_width, 'kv', axis=0, tiled=True), weight_cols...  2.06 us
  transfers between devices with their start and end apart: 1, of which 0 were waited for; matrix products, arithmetic and copies ran while one was open for 20% of the time, Pallas kernels for 0%

commit v1 on v0

--- a/solution.py
+++ b/solution.py
@@ -59,7 +59,7 @@
     mixed_rows = jnp.stack(outputs, axis=1).reshape(row_count, local_width)
     gated_rows = mixed_rows.astype(jnp.bfloat16)
     weight_cols = lax.all_gather(output_matrix, "tp", axis=0, tiled=True)
-    full_width = lax.all_gather(gated_rows, "tp", axis=1, tiled=True)
+    full_width = jnp.concatenate(lax.all_gather(gated_rows, "tp"), axis=1)
     every_row = jnp.dot(
         lax.all_gather(full_width, "kv", axis=0, tiled=True),
         weight_cols,

time: 77.7 us -> 77.7 us (level)
  no operation moved by 1% of the time
where the time goes in v1:
time: 77.7 us; the launch traced here: 77.3 us
  blocking collectives  43.4 us (56%)
  between operations  14.3 us (18%)
  matrix products  11.1 us (14%)
  other arithmetic  5.54 us (7%)
  local copies, waits for them, and re-layouts  2.29 us (3%)
    all_gather x1, blocking collectives, per_device(): lax.all_gather(full_width, 'kv', axis=0, tiled=True)  31.2 us
    dot_general x3, matrix products, project(): jnp.dot(scaled, weight, preferred_element_type=jnp.float32) * row_scale  6.72 us
    all_gather x1, blocking collectives, per_device(): whole = lax.all_gather(proposals, 'tp', axis=2, tiled=True)  6.44 us
    all_gather x1, blocking collectives, per_device(): full_width = jnp.concatenate(lax.all_gather(gated_rows, 'tp'), axis=1)  5.78 us
    dot_general x4, matrix products, per_device(): outputs.append(jnp.einsum('shvk,shk->shv', carried, query_act[:, position]))  2.3 us
    dot_general x1, matrix products, per_device(): jnp.dot(lax.all_gather(full_width, 'kv', axis=0, tiled=True), weight_cols...  2.06 us
  transfers between devices with their start and end apart: 1, of which 0 were waited for; matrix products, arithmetic and copies ran while one was open for 20% of the time, Pallas kernels for 0%

profile of v1, /device:TPU:0, one launch (start us, length us, event | category | flops | bytes accessed | tf_op | source)
XLA Modules:
  0.0 77.3 jit_solution(6080502227691796647)
XLA Ops:
  7.2 0.0 copy-start
  7.2 0.0 all-gather.2.cloned.1.call-start
  7.2 0.7 all-gather.2.cloned.1.call-update
  7.9 0.7 compare_and_fusion
  8.6 0.7 fusion.44
  9.2 6.4 %all_gather.13 = bf16[2,4,4096]{2,1,0:T(4,128)(2,1)S(1)} all-gather(bf16[2,4,1024]{2,1,0:T(4,128)(2,1)} %param.10), channel_id=1, replica_groups=mesh['kv'=8,'tp'=4] {'tp'}, dimensions={2}, use_global_device_ids=true | all-gather | bytes 81920 | tf_op jit(solution)/shard_map/all_gather | solution.py:21
  15.7 0.1 multiply_reduce_fusion
  15.9 0.1 copy.14
  15.9 0.2 or_reduce_fusion
  16.1 0.7 broadcast_subtract_fusion
  16.8 0.1 rsqrt.11
  16.9 0.7 multiply_convert_fusion
  17.7 3.1 %divide_multiply_fusion = f32[8,512]{1,0:T(8,128)S(1)} fusion(bf16[8,4096]{1,0:T(8,128)(2,1)S(1)} %multiply_convert_fusion, bf16[4096,512]{1,0:T(8,128)(2,1)} %param.12, f32[8]{0:T(128)S(1)} %rsqrt.11), kind=kOutput, calls=%fused_computation.58 | convolution fusion | flops 33583104 | bytes 4276256 | tf_op jit(solution)/shard_map/dot_general | solution.py:27
  20.8 0.0 copy-start.1
  20.8 2.9 %fusion.7 = f32[8,512]{1,0:T(8,128)S(1)} fusion(bf16[8,4096]{1,0:T(8,128)(2,1)S(1)} %multiply_convert_fusion, bf16[4096,512]{1,0:T(8,128)(2,1)} %param.14, f32[8]{0:T(128)S(1)} %rsqrt.11), kind=kOutput, calls=%fused_computation.12 | convolution fusion | flops 33566720 | bytes 4276256 | tf_op jit(solution)/shard_map/dot_general | solution.py:27
  23.8 0.5 copy-done.1
  24.3 0.0 copy-start.2
  24.3 0.0 copy-start.3
  24.3 0.7 fusion.5
  25.0 0.0 copy-done.2
  25.0 0.0 copy-done.3
  25.0 0.1 log_add_fusion
  25.1 0.0 copy-done
  25.1 0.6 gather_fusion
  25.7 0.3 fusion.45
  26.0 0.5 fusion.19
  26.5 0.6 fusion.20
  27.1 0.9 %fusion.15 = f32[2,4,1,128]{3,2,1,0:T(1,128)S(1)} fusion(f32[2,4,128,1]{2,3,1,0:T(1,128)S(1)} %bitcast.169, f32[2,4,128]{2,1,0:T(4,128)S(1)} %get-tuple-element.24, f32[2,4,128]{2,1,0:T(4,128)S(1)} %get-tuple-element.11, f32[2,4,128]{2,1,0:T(4,128)S(1)} %get-tuple-element.29, f32[2,4,128]{2,1,0:T(4,128)S(1)} %get-tuple-element.25, ...), kind=kOutput, calls=%fused_computation.28 | convolution fusion | flops 1966080 | bytes 581634 | tf_op jit(solution)/shard_map/shvk,shk->shv/dot_general | solution.py:57
  28.1 5.8 %all_gather.14 = bf16[4,8,512]{2,1,0:T(8,128)(2,1)S(1)} all-gather(bf16[1,8,512]{2,1,0:T(8,128)(2,1)S(1)} %convert_element_type.51), channel_id=1, replica_groups=mesh['kv'=8,'tp'=4] {'tp'}, dimensions={0}, use_global_device_ids=true | all-gather | bytes 40960 | tf_op jit(solution)/shard_map/all_gather | solution.py:62
  33.8 31.2 %all_gather.15 = bf16[64,2048]{1,0:T(8,128)(2,1)S(1)} all-gather(bf16[8,2048]{1,0:T(8,128)(2,1)S(1)} %bitcast.162), channel_id=1, replica_groups=mesh['kv'=8,'tp'=4] {'kv'}, dimensions={0}, use_global_device_ids=true | all-gather | bytes 294912 | tf_op jit(solution)/shard_map/all_gather | solution.py:64
  65.3 0.5 fusion.11
  66.0 0.4 fusion.10
  66.3 1.5 %pad_maximum_fusion = f32[2,4,512,128]{3,2,1,0:T(8,128)} fusion(f32[2,1,512,128]{3,2,1,0:T(8,128)S(1)} %fusion.10, f32[2,1,512,128]{3,2,1,0:T(8,128)S(1)} %get-tuple-element.2, f32[2,1,512,128]{3,2,1,0:T(8,128)S(1)} %get-tuple-element.3, f32[2,1,512,128]{3,2,1,0:T(8,128)S(1)} %get-tuple-element.4), kind=kLoop, calls=%fused_computation.1 | loop fusion | flops 1572864 | bytes 4194304 | tf_op jit(solution)/shard_map/stack | solution.py:74
  67.8 0.0 all-gather.2.cloned.1.call-done
  67.8 2.1 %fusion.49 = bf16[64,512]{1,0:T(8,128)(2,1)S(1)} fusion(bf16[64,2048]{1,0:T(8,128)(2,1)S(1)} %all_gather.15, bf16[2048,512]{1,0:T(8,128)(2,1)} %all-gather.2.cloned.1.call-done), kind=kOutput, calls=%fused_computation.100 | convolution fusion | flops 134217728 | bytes 2424832 | tf_op jit(solution)/shard_map/dot_general | solution.py:63
  69.9 0.6 reshape.337
  (27 shorter events, 0.5 us)
Async XLA Ops:
  7.2 17.9 %copy-start = (f32[2,4,512,128]{3,2,1,0:T(8,128)S(1)}, f32[2,4,512,128]{3,2,1,0:T(8,128)}, u32[]{:S(2)}) copy-start(f32[2,4,512,128]{3,2,1,0:T(8,128)} %param.17) | copy-start | bytes 6291460
  7.2 60.6 %all-gather.2.cloned.1.call-start = ((), (), s32[]{:S(2)}) async-start(), calls=%async_computation | async-start | bytes 2621440 | tf_op jit(solution)/shard_map/all_gather | solution.py:61
  20.8 3.5 %copy-start.1 = (bf16[4096,512]{1,0:T(8,128)(2,1)S(1)}, bf16[4096,512]{1,0:T(8,128)(2,1)}, u32[]{:S(2)}) copy-start(bf16[4096,512]{1,0:T(8,128)(2,1)} %param.13) | copy-start | bytes 12582916
  24.3 0.7 copy-start.2
  24.3 0.7 copy-start.3
Sparse Core Ops, SparseCore 0:
  9.5 25.4 all-gather.1
